TPU v7x, 32 devices: a whole 2x2x4 slice. The times are simulated.
32 devices in a mesh: sp: 8 (over z, x), dp: 4 (over y, core).
Axes of the slice: x: 2, y: 2, z: 4, core: 2. Of those that a mesh axis runs over, the one named last changes fastest.
Arguments:
- gate_in: bfloat16 [4, 4096, 1024], P('dp', 'sp'), may hold values from -6 to 6
- value_in: bfloat16 [4, 4096, 1024], P('dp', 'sp'), may hold values from -6 to 6
- segments: int32 [4, 4096], P('dp', 'sp'), may hold values from 0 to 1, never falling along the last dimension, each value on 1 to 3072 neighbouring positions
- value_gain: bfloat16 [1024], P('sp'), may hold values from 0.099609375 to 1.8984375
- mixing: bfloat16 [8, 1024, 1024], P('sp', 'dp'), may hold values from -0.1875 to 0.1875
- mixing_bias: bfloat16 [8, 1024], P('sp'), may hold values from 0.099609375 to 1.8984375
Outputs:
- gated: bfloat16 [4, 4096, 1024], P('dp', 'sp')
Inputs may be any that keep to these rules, and one draw needn't show every extreme that they name: `segments`: within each sequence the numbers never fall, every number 0 to 1 occurs, a document spans at most 3072 positions and some document spans exactly that.
All inputs are finite; a program needn't handle non-finite values.
Results may differ from a plain program's by a relative error of at most 0.0054.
Values may be sent and summed in bfloat16 or wider, within the bound.
No kernel may reach another device: no remote copies, remote signals or barrier semaphores. Data moves between devices by JAX's collectives and lax.ppermute only.
A program may use at most 128 MiB of HBM per device.

v0:
```python
import jax
import jax.numpy as jnp
from jax import lax
from jax.sharding import PartitionSpec as P

HEAD_DIM = 128
epsilon = 1e-06


def head_norm(values, gain_f, head_dim):
    shaped = values.reshape(values.shape[:-1] + (values.shape[-1] // head_dim, head_dim))
    scaled = shaped * lax.rsqrt(jnp.mean(shaped * shaped, axis=-1, keepdims=True) + epsilon)
    return (scaled.reshape(values.shape) * gain_f).astype(jnp.bfloat16)


def per_device(gate_in, value_in, segments, value_gain, mixing, mixing_bias):
    sp_count = lax.axis_size("sp")
    sequences = value_in.shape[0]
    tokens = value_in.shape[1]
    length = tokens * sp_count
    block_len = mixing.shape[2]
    heads_here = mixing.shape[0]
    head_dim = HEAD_DIM
    id_tile = jnp.broadcast_to(
        segments.astype(jnp.bfloat16)[:, :, None], (sequences, tokens, sp_count)
    )
    value_heads, id_heads = (
        lax.all_to_all(value_in, "sp", split_axis=2, concat_axis=1, tiled=True),
        lax.all_to_all(id_tile, "sp", split_axis=2, concat_axis=1, tiled=True),
    )
    gain_f = value_gain.astype(jnp.float32)
    normed = head_norm(jax.nn.gelu(value_heads.astype(jnp.float32)), gain_f, head_dim)
    blocks = sequences * length // block_len
    value_blocks = normed.reshape(blocks, block_len, heads_here, head_dim)
    id_blocks = id_heads.reshape(blocks, block_len)
    bias_f = mixing_bias.astype(jnp.float32)
    nothing = jnp.zeros((), jnp.bfloat16)
    shard_piece = lax.all_gather(mixing, "dp", axis=1, tiled=True)
    bias_rows = jnp.transpose(bias_f)[:, :, None]

    def one_block(pair_item):
        block_values, block_ids = pair_item
        same_doc = block_ids[:, None] == block_ids[None, :]
        masked = jnp.where(same_doc[None, :, :], shard_piece, nothing)
        summed = jnp.einsum(
            "hts,shd->thd", masked, block_values, preferred_element_type=jnp.float32
        )
        return (summed + bias_rows).astype(jnp.bfloat16)

    mixed = lax.map(one_block, (value_blocks, id_blocks))
    mixed = mixed.reshape(sequences, length, heads_here * head_dim)
    returned = lax.all_to_all(mixed, "sp", split_axis=1, concat_axis=2, tiled=True)
    return (jax.nn.gelu(gate_in.astype(jnp.float32)) * returned.astype(jnp.float32)).astype(
        jnp.bfloat16
    )


def solution(mesh):
    return jax.shard_map(
        per_device,
        mesh=mesh,
        in_specs=(
            P("dp", "sp", None),
            P("dp", "sp", None),
            P("dp", "sp"),
            P("sp"),
            P("sp", "dp", None),
            P("sp", None),
        ),
        out_specs=P("dp", "sp", None),
        check_vma=False,
    )
```

profile of v0, /device:TPU:0, one launch (start us, length us, event | category | flops | bytes accessed | tf_op | source)
XLA Modules:
  0.0 162.7 jit_solution(6695371021300023633)
XLA Ops:
  6.5 0.7 all-gather.2.cloned.1.call-update
  7.3 0.7 convert_reduce_fusion
  8.0 0.5 broadcast.193
  8.5 0.6 reduce.7
  9.0 0.6 reshape.283
  9.7 7.3 %all-to-all-start.1 = ((bf16[8,2,256]{2,1,0:T(2,128)(2,1)}), bf16[8,2,256]{2,1,0:T(2,128)(2,1)S(1)}, u32[]{:S(2)}, u32[]{:S(2)}) async-start(bf16[8,2,256]{2,1,0:T(2,128)(2,1)} %reshape.283), calls=%async_computation.1 | async-start | bytes 16384 | tf_op jit(solution)/shard_map/all_to_all | solution.py:29
  16.9 4.7 %copy.44 = bf16[1,512,1024]{1,0,2:T(2,128)(2,1)S(1)} copy(bf16[1,512,1024]{2,1,0:T(8,128)(2,1)} %param.9) | data formatting | bytes 2097152 | tf_op args[1]
  21.6 6.9 %reduce.6 = bf16[1024,512]{1,0:T(8,128)(2,1)S(1)} reduce(bf16[1024,1,512]{2,1,0:T(2,128)(2,1)S(1)} %bitcast.83, bf16[]{:T(256)} %broadcast.193), dimensions={1}, to_apply=%bitcast.59.reduce_sub_computation | reduce | bytes 2097154
  28.6 1.6 reshape.281
  30.2 6.0 %all-to-all-start = ((bf16[8,2,32768]{2,1,0:T(2,128)(2,1)}), bf16[8,2,32768]{2,1,0:T(2,128)(2,1)S(1)}, u32[]{:S(2)}, u32[]{:S(2)}) async-start(bf16[8,2,32768]{2,1,0:T(2,128)(2,1)} %reshape.281), calls=%async_computation | async-start | bytes 2097152 | tf_op jit(solution)/shard_map/all_to_all | solution.py:28
  36.3 25.3 %all-to-all-done = bf16[8,2,32768]{2,1,0:T(2,128)(2,1)S(1)} async-done(((bf16[8,2,32768]{2,1,0:T(2,128)(2,1)}), bf16[8,2,32768]{2,1,0:T(2,128)(2,1)S(1)}, u32[]{:S(2)}, u32[]{:S(2)}) %all-to-all-start) | async-done | bytes 1048608 | tf_op jit(solution)/shard_map/all_to_all | solution.py:28
  61.6 1.0 reshape.282
  62.6 0.3 copy.45
  62.9 0.5 copy.46
  63.5 0.8 fusion.47
  64.4 1.7 %fusion.31 = bf16[4,1024,1,128]{3,1,2,0:T(8,128)(2,1)} fusion(f32[4,1024,1,128]{3,1,2,0:T(8,128)S(1)} %bitcast.79, f32[128]{0:T(128)S(1)} %convert_element_type.89, f32[4,1024]{1,0:T(4,128)S(1)} %rsqrt.12), kind=kLoop, calls=%fused_computation.31 | loop fusion | flops 5767168 | bytes 3162624 | tf_op jit(solution)/shard_map/convert_element_type | solution.py:13
  66.0 11.5 %while.10 = (s32[]{:T(128)}, bf16[4,1024,1,128]{3,1,0,2:T(8,128)(2,1)S(1)}, bf16[4,1024,1,128]{3,1,2,0:T(8,128)(2,1)}, bf16[4,1024]{1,0:T(4,128)(2,1)S(1)}, bf16...) while((s32[]{:T(128)}, bf16[4,1024,1,128]{3,1,0,2:T(8,128)(2,1)S(1)}, ...), condition=%wide.region_2.3_spmd, body=%wide.region_1.2_spmd.sunk | while | flops 270794752 | bytes 3682901 | solution.py:50
  66.1 2.6 %fusion.53 = bf16[1,1024,1,128]{1,3,2,0:T(8,128)(2,1)S(1)} fusion(bf16[1,1024,1024]{2,1,0:T(8,128)(2,1)} %get-tuple-element.105, bf16[1024]{0:T(1024)(128)(2,1)S(1)} %dynamic-slice_reduce_fusion.2, f32[1024]{0:T(1024)S(1)} %bitcast.89, bf16[4,1024,1,128]{3,1,2,0:T(8,128)(2,1)} %get-tuple-element.103, s32[]{:T(128)} %get-tuple-element.94), kind=kOutput, calls=%fused_computation.6.clone.1 | convolution fusion | flops 270794752 | bytes 2630144 | tf_op jit(solution)/shard_map/while/body/eval_jaxpr/hts,shd->thd/dot_general | solution.py:45
  69.0 2.6 %fusion.53 = bf16[1,1024,1,128]{1,3,2,0:T(8,128)(2,1)S(1)} fusion(bf16[1,1024,1024]{2,1,0:T(8,128)(2,1)} %get-tuple-element.105, bf16[1024]{0:T(1024)(128)(2,1)S(1)} %dynamic-slice_reduce_fusion.2, f32[1024]{0:T(1024)S(1)} %bitcast.89, bf16[4,1024,1,128]{3,1,2,0:T(8,128)(2,1)} %get-tuple-element.103, s32[]{:T(128)} %get-tuple-element.94), kind=kOutput, calls=%fused_computation.6.clone.1 | convolution fusion | flops 270794752 | bytes 2630144 | tf_op jit(solution)/shard_map/while/body/eval_jaxpr/hts,shd->thd/dot_general | solution.py:45
  71.8 2.6 %fusion.53 = bf16[1,1024,1,128]{1,3,2,0:T(8,128)(2,1)S(1)} fusion(bf16[1,1024,1024]{2,1,0:T(8,128)(2,1)} %get-tuple-element.105, bf16[1024]{0:T(1024)(128)(2,1)S(1)} %dynamic-slice_reduce_fusion.2, f32[1024]{0:T(1024)S(1)} %bitcast.89, bf16[4,1024,1,128]{3,1,2,0:T(8,128)(2,1)} %get-tuple-element.103, s32[]{:T(128)} %get-tuple-element.94), kind=kOutput, calls=%fused_computation.6.clone.1 | convolution fusion | flops 270794752 | bytes 2630144 | tf_op jit(solution)/shard_map/while/body/eval_jaxpr/hts,shd->thd/dot_general | solution.py:45
  74.7 2.6 %fusion.53 = bf16[1,1024,1,128]{1,3,2,0:T(8,128)(2,1)S(1)} fusion(bf16[1,1024,1024]{2,1,0:T(8,128)(2,1)} %get-tuple-element.105, bf16[1024]{0:T(1024)(128)(2,1)S(1)} %dynamic-slice_reduce_fusion.2, f32[1024]{0:T(1024)S(1)} %bitcast.89, bf16[4,1024,1,128]{3,1,2,0:T(8,128)(2,1)} %get-tuple-element.103, s32[]{:T(128)} %get-tuple-element.94), kind=kOutput, calls=%fused_computation.6.clone.1 | convolution fusion | flops 270794752 | bytes 2630144 | tf_op jit(solution)/shard_map/while/body/eval_jaxpr/hts,shd->thd/dot_general | solution.py:45
  77.6 16.7 %copy.63 = bf16[1,4096,128]{2,0,1:T(2,128)(2,1)S(1)} copy(bf16[1,4096,128]{2,1,0:T(8,128)(2,1)S(1)} %bitcast.86) | data formatting | bytes 2097152 | tf_op jit(solution)/shard_map/reshape | solution.py:51
  94.3 22.3 %reduce.8 = bf16[4096,128]{1,0:T(8,128)(2,1)S(1)} reduce(bf16[4096,1,128]{2,1,0:T(2,128)(2,1)S(1)} %bitcast.82, bf16[]{:T(256)} %broadcast.193), dimensions={1}, to_apply=%bitcast.68.reduce_sub_computation | reduce | bytes 2097154
  116.6 1.1 reshape.285
  117.7 3.6 %all-to-all-start.2 = ((bf16[8,2,32768]{2,1,0:T(2,128)(2,1)}), bf16[8,2,32768]{2,1,0:T(2,128)(2,1)S(1)}, u32[]{:S(2)}, u32[]{:S(2)}) async-start(bf16[8,2,32768]{2,1,0:T(2,128)(2,1)} %reshape.285), calls=%async_computation.2 | async-start | bytes 2097152 | tf_op jit(solution)/shard_map/all_to_all | solution.py:52
  121.3 1.3 copy.43
  122.6 24.4 %all-to-all-done.2 = bf16[8,2,32768]{2,1,0:T(2,128)(2,1)S(1)} async-done(((bf16[8,2,32768]{2,1,0:T(2,128)(2,1)}), bf16[8,2,32768]{2,1,0:T(2,128)(2,1)S(1)}, u32[]{:S(2)}, u32[]{:S(2)}) %all-to-all-start.2) | async-done | bytes 1048608 | tf_op jit(solution)/shard_map/all_to_all | solution.py:52
  147.1 1.0 reshape.286
  148.3 1.5 convert_bitcast_fusion
  149.8 2.0 %copy.55 = f32[1,512,8,128]{1,3,2,0:T(8,128)S(1)} copy(f32[1,512,8,128]{3,1,2,0:T(8,128)} %convert_bitcast_fusion) | data formatting | bytes 4194304 | tf_op jit(solution)/shard_map/convert_element_type | solution.py:53
  151.8 1.8 %fusion.46 = bf16[1,512,1024]{1,2,0:T(8,128)(2,1)} fusion(bf16[1,512,1024]{1,2,0:T(8,128)(2,1)S(1)} %copy-done, f32[1,512,8,128]{1,3,2,0:T(8,128)S(1)} %copy.55), kind=kLoop, calls=%fused_computation.46 | loop fusion | flops 5767168 | bytes 4194304 | tf_op jit(solution)/shard_map/convert_element_type | solution.py:53
  153.6 2.3 %copy.56 = bf16[1,512,1024]{2,1,0:T(8,128)(2,1)} copy(bf16[1,512,1024]{1,2,0:T(8,128)(2,1)} %fusion.46) | data formatting | bytes 2097152 | tf_op jit(solution)/shard_map/convert_element_type | solution.py:53
  (35 shorter events, 1.2 us)
Async XLA Ops:
  6.5 59.5 %all-gather.2.cloned.1.call-start = ((), (), s32[]{:S(2)}) async-start(), calls=%async_computation.3 | async-start | bytes 2621440 | tf_op jit(solution)/shard_map/all_gather | solution.py:38
  9.7 20.5 %all-to-all-start.1 = ((bf16[8,2,256]{2,1,0:T(2,128)(2,1)}), bf16[8,2,256]{2,1,0:T(2,128)(2,1)S(1)}, u32[]{:S(2)}, u32[]{:S(2)}) async-start(bf16[8,2,256]{2,1,0:T(2,128)(2,1)} %reshape.283), calls=%async_computation.1 | async-start | bytes 16384 | tf_op jit(solution)/shard_map/all_to_all | solution.py:29
  28.6 7.6 %copy-start.4 = (bf16[128]{0:T(256)(128)(2,1)S(1)}, bf16[128]{0:T(256)(128)(2,1)}, u32[]{:S(2)}) copy-start(bf16[128]{0:T(256)(128)(2,1)} %param.11) | copy-start | bytes 772
  28.6 7.6 %copy-start.3 = (bf16[1,1024]{1,0:T(2,128)(2,1)S(1)}, bf16[1,1024]{1,0:T(2,128)(2,1)}, u32[]{:S(2)}) copy-start(bf16[1,1024]{1,0:T(2,128)(2,1)} %param.13) | copy-start | bytes 6148
  30.2 31.4 %all-to-all-start = ((bf16[8,2,32768]{2,1,0:T(2,128)(2,1)}), bf16[8,2,32768]{2,1,0:T(2,128)(2,1)S(1)}, u32[]{:S(2)}, u32[]{:S(2)}) async-start(bf16[8,2,32768]{2,1,0:T(2,128)(2,1)} %reshape.281), calls=%async_computation | async-start | bytes 2097152 | tf_op jit(solution)/shard_map/all_to_all | solution.py:28
  64.3 1.7 %copy-start.1 = (bf16[4,1024,1,128]{3,1,0,2:T(8,128)(2,1)S(1)}, bf16[4,1024,1,128]{3,1,0,2:T(8,128)(2,1)}, u32[]{:S(2)}) copy-start(bf16[4,1024,1,128]{3,1,0,2:T(8,128)(2,1)} %custom-call) | copy-start | bytes 3145732
  116.6 4.7 %copy-start.2 = (bf16[1,512,1024]{2,1,0:T(8,128)(2,1)S(1)}, bf16[1,512,1024]{2,1,0:T(8,128)(2,1)}, u32[]{:S(2)}) copy-start(bf16[1,512,1024]{2,1,0:T(8,128)(2,1)} %param.8) | copy-start | bytes 3145732
  117.7 29.3 %all-to-all-start.2 = ((bf16[8,2,32768]{2,1,0:T(2,128)(2,1)}), bf16[8,2,32768]{2,1,0:T(2,128)(2,1)S(1)}, u32[]{:S(2)}, u32[]{:S(2)}) async-start(bf16[8,2,32768]{2,1,0:T(2,128)(2,1)} %reshape.285), calls=%async_computation.2 | async-start | bytes 2097152 | tf_op jit(solution)/shard_map/all_to_all | solution.py:52
  149.8 2.0 %copy-start = (bf16[1,512,1024]{1,2,0:T(8,128)(2,1)S(1)}, bf16[1,512,1024]{1,2,0:T(8,128)(2,1)}, u32[]{:S(2)}) copy-start(bf16[1,512,1024]{1,2,0:T(8,128)(2,1)} %copy.43) | copy-start | bytes 3145732
Sparse Core Ops, SparseCore 0:
  8.9 25.2 all-gather.1
where the time goes:
time: 163 us
  waiting for transfers between devices  50.5 us (31%)
  other arithmetic  36.3 us (22%)
  local copies, waits for them, and re-layouts  34.9 us (21%)
  starting transfers between devices  16.8 us (10%)
  between operations  13.6 us (8%)
  matrix products  10.4 us (6%)
    unnamed x3, other arithmetic  29.8 us
    all_to_all x1, waiting for transfers between devices, per_device(): lax.all_to_all(value_in, 'sp', split_axis=2, concat_axis=1, tiled=True)  25.3 us
    all_to_all x1, waiting for transfers between devices, per_device(): lax.all_to_all(mixed, 'sp', split_axis=1, concat_axis=2, tiled=True)  24.4 us
    reshape x1, local copies, waits for them, and re-layouts, per_device(): mixed = mixed.reshape(sequences, length, heads_here * head_dim)  16.7 us
    unnamed x21, local copies, waits for them, and re-layouts  11.9 us
    dot_general x4, matrix products, one_block(): jnp.einsum('hts,shd->thd', masked, block_values, preferred_element_type=j...  10.4 us
    all_to_all x1, starting transfers between devices, per_device(): lax.all_to_all(id_tile, 'sp', split_axis=2, concat_axis=1, tiled=True)  7.28 us
    all_to_all x1, starting transfers between devices, per_device(): lax.all_to_all(value_in, 'sp', split_axis=2, concat_axis=1, tiled=True)  5.99 us
  transfers between devices with their start and end apart: 4, of which 2 were waited for; matrix products, arithmetic and copies ran while one was open for 13% of the time, Pallas kernels for 0%

commit v1 on v0

--- a/solution.py
+++ b/solution.py
@@ -49,7 +49,10 @@
 
     mixed = lax.map(one_block, (value_blocks, id_blocks))
     mixed = mixed.reshape(sequences, length, heads_here * head_dim)
-    returned = lax.all_to_all(mixed, "sp", split_axis=1, concat_axis=2, tiled=True)
+    returned = jnp.concatenate(
+        lax.all_to_all(jnp.stack(jnp.split(mixed, lax.psum(1, "sp"), axis=1), axis=0), "sp", 0, 0),
+        axis=2,
+    )
     return (jax.nn.gelu(gate_in.astype(jnp.float32)) * returned.astype(jnp.float32)).astype(
         jnp.bfloat16
     )

time: 163 us -> 127 us (0.78)
  other arithmetic: 36.3 us -> 14.2 us
  local copies, waits for them, and re-layouts: 34.9 us -> 20.3 us
    unnamed x3 -> x2, other arithmetic: 29.8 us -> 7.68 us
    reshape x1 -> x0, local copies, waits for them, and re-layouts: 16.7 us -> none  [per_device(): mixed = mixed.reshape(sequences, length, heads_here * head_dim)]
    unnamed x21 -> x24, local copies, waits for them, and re-layouts: 11.9 us -> 13.7 us
  transfers between devices with their start and end apart: 4 -> 4, of which waited for: 2 -> 2; matrix products, arithmetic and copies ran while one was open for 13% -> 16% of each run, Pallas kernels for 0% -> 0%
where the time goes in v1:
time: 127 us
  waiting for transfers between devices  51.2 us (40%)
  local copies, waits for them, and re-layouts  20.3 us (16%)
  starting transfers between devices  16.8 us (13%)
  other arithmetic  14.2 us (11%)
  between operations  13.6 us (11%)
  matrix products  10.4 us (8%)
    all_to_all x1, waiting for transfers between devices, per_device(): lax.all_to_all(value_in, 'sp', split_axis=2, concat_axis=1, tiled=True)  25.3 us
    all_to_all x1, waiting for transfers between devices, per_device(): lax.all_to_all(jnp.stack(jnp.split(mixed, lax.psum(1, 'sp'), axis=1), axi...  25.2 us
    unnamed x24, local copies, waits for them, and re-layouts  13.7 us
    dot_general x4, matrix products, one_block(): jnp.einsum('hts,shd->thd', masked, block_values, preferred_element_type=j...  10.4 us
    unnamed x2, other arithmetic  7.68 us
    all_to_all x1, starting transfers between devices, per_device(): lax.all_to_all(id_tile, 'sp', split_axis=2, concat_axis=1, tiled=True)  7.28 us
    all_to_all x1, starting transfers between devices, per_device(): lax.all_to_all(value_in, 'sp', split_axis=2, concat_axis=1, tiled=True)  5.99 us
    all_to_all x1, starting transfers between devices, per_device(): lax.all_to_all(jnp.stack(jnp.split(mixed, lax.psum(1, 'sp'), axis=1), axi...  3.56 us
  transfers between devices with their start and end apart: 4, of which 2 were waited for; matrix products, arithmetic and copies ran while one was open for 16% of the time, Pallas kernels for 0%

profile of v1, /device:TPU:0, one launch (start us, length us, event | category | flops | bytes accessed | tf_op | source)
XLA Modules:
  0.0 126.7 jit_solution(86155714421104263)
XLA Ops:
  6.5 0.7 all-gather.2.cloned.1.call-update
  7.3 0.7 convert_reduce_fusion
  8.5 0.7 reduce.7
  9.2 0.6 reshape.282
  9.8 7.3 %all-to-all-start.1 = ((bf16[8,2,256]{2,1,0:T(2,128)(2,1)}), bf16[8,2,256]{2,1,0:T(2,128)(2,1)S(1)}, u32[]{:S(2)}, u32[]{:S(2)}) async-start(bf16[8,2,256]{2,1,0:T(2,128)(2,1)} %reshape.282), calls=%async_computation.1 | async-start | bytes 16384 | tf_op jit(solution)/shard_map/all_to_all | solution.py:29
  17.1 4.7 %copy.45 = bf16[1,512,1024]{1,0,2:T(2,128)(2,1)S(1)} copy(bf16[1,512,1024]{2,1,0:T(8,128)(2,1)} %param.9) | data formatting | bytes 2097152 | tf_op args[1]
  21.7 7.0 %reduce.6 = bf16[1024,512]{1,0:T(8,128)(2,1)S(1)} reduce(bf16[1024,1,512]{2,1,0:T(2,128)(2,1)S(1)} %bitcast.107, bf16[]{:T(256)} %broadcast.193), dimensions={1}, to_apply=%bitcast.89.reduce_sub_computation | reduce | bytes 2097154
  28.8 1.6 %reshape.280 = bf16[8,2,32768]{2,1,0:T(2,128)(2,1)} reshape(bf16[1024,512]{1,0:T(8,128)(2,1)S(1)} %reduce.6) | data formatting | bytes 2097152
  30.4 6.0 %all-to-all-start = ((bf16[8,2,32768]{2,1,0:T(2,128)(2,1)}), bf16[8,2,32768]{2,1,0:T(2,128)(2,1)S(1)}, u32[]{:S(2)}, u32[]{:S(2)}) async-start(bf16[8,2,32768]{2,1,0:T(2,128)(2,1)} %reshape.280), calls=%async_computation | async-start | bytes 2097152 | tf_op jit(solution)/shard_map/all_to_all | solution.py:28
  36.5 25.3 %all-to-all-done = bf16[8,2,32768]{2,1,0:T(2,128)(2,1)S(1)} async-done(((bf16[8,2,32768]{2,1,0:T(2,128)(2,1)}), bf16[8,2,32768]{2,1,0:T(2,128)(2,1)S(1)}, u32[]{:S(2)}, u32[]{:S(2)}) %all-to-all-start) | async-done | bytes 1048608 | tf_op jit(solution)/shard_map/all_to_all | solution.py:28
  61.8 1.0 reshape.281
  63.6 0.8 fusion.47
  64.5 1.7 %fusion.31 = bf16[4,1024,1,128]{3,1,2,0:T(8,128)(2,1)} fusion(f32[4,1024,1,128]{3,1,2,0:T(8,128)S(1)} %bitcast.105, f32[128]{0:T(128)S(1)} %convert_element_type.86, f32[4,1024]{1,0:T(4,128)S(1)} %rsqrt.12), kind=kLoop, calls=%fused_computation.31 | loop fusion | flops 5767168 | bytes 3162624 | tf_op jit(solution)/shard_map/convert_element_type | solution.py:13
  66.2 11.5 %while.10 = (s32[]{:T(128)}, bf16[4,1024,1,128]{3,1,0,2:T(8,128)(2,1)S(1)}, bf16[4,1024,1,128]{3,1,2,0:T(8,128)(2,1)}, bf16[4,1024]{1,0:T(4,128)(2,1)S(1)}, bf16...) while((s32[]{:T(128)}, bf16[4,1024,1,128]{3,1,0,2:T(8,128)(2,1)S(1)}, ...), condition=%wide.region_2.3_spmd, body=%wide.region_1.2_spmd.sunk | while | flops 270794752 | bytes 3682901 | solution.py:50
  66.2 2.6 %fusion.61 = bf16[1,1024,1,128]{1,3,2,0:T(8,128)(2,1)S(1)} fusion(bf16[1,1024,1024]{2,1,0:T(8,128)(2,1)} %get-tuple-element.105, bf16[1024]{0:T(1024)(128)(2,1)S(1)} %dynamic-slice_reduce_fusion.2, f32[1024]{0:T(1024)S(1)} %bitcast.119, bf16[4,1024,1,128]{3,1,2,0:T(8,128)(2,1)} %get-tuple-element.103, s32[]{:T(128)} %get-tuple-element.94), kind=kOutput, calls=%fused_computation.6.clone.1 | convolution fusion | flops 270794752 | bytes 2630144 | tf_op jit(solution)/shard_map/while/body/eval_jaxpr/hts,shd->thd/dot_general | solution.py:45
  69.1 2.6 %fusion.61 = bf16[1,1024,1,128]{1,3,2,0:T(8,128)(2,1)S(1)} fusion(bf16[1,1024,1024]{2,1,0:T(8,128)(2,1)} %get-tuple-element.105, bf16[1024]{0:T(1024)(128)(2,1)S(1)} %dynamic-slice_reduce_fusion.2, f32[1024]{0:T(1024)S(1)} %bitcast.119, bf16[4,1024,1,128]{3,1,2,0:T(8,128)(2,1)} %get-tuple-element.103, s32[]{:T(128)} %get-tuple-element.94), kind=kOutput, calls=%fused_computation.6.clone.1 | convolution fusion | flops 270794752 | bytes 2630144 | tf_op jit(solution)/shard_map/while/body/eval_jaxpr/hts,shd->thd/dot_general | solution.py:45
  72.0 2.6 %fusion.61 = bf16[1,1024,1,128]{1,3,2,0:T(8,128)(2,1)S(1)} fusion(bf16[1,1024,1024]{2,1,0:T(8,128)(2,1)} %get-tuple-element.105, bf16[1024]{0:T(1024)(128)(2,1)S(1)} %dynamic-slice_reduce_fusion.2, f32[1024]{0:T(1024)S(1)} %bitcast.119, bf16[4,1024,1,128]{3,1,2,0:T(8,128)(2,1)} %get-tuple-element.103, s32[]{:T(128)} %get-tuple-element.94), kind=kOutput, calls=%fused_computation.6.clone.1 | convolution fusion | flops 270794752 | bytes 2630144 | tf_op jit(solution)/shard_map/while/body/eval_jaxpr/hts,shd->thd/dot_general | solution.py:45
  74.9 2.6 %fusion.61 = bf16[1,1024,1,128]{1,3,2,0:T(8,128)(2,1)S(1)} fusion(bf16[1,1024,1024]{2,1,0:T(8,128)(2,1)} %get-tuple-element.105, bf16[1024]{0:T(1024)(128)(2,1)S(1)} %dynamic-slice_reduce_fusion.2, f32[1024]{0:T(1024)S(1)} %bitcast.119, bf16[4,1024,1,128]{3,1,2,0:T(8,128)(2,1)} %get-tuple-element.103, s32[]{:T(128)} %get-tuple-element.94), kind=kOutput, calls=%fused_computation.6.clone.1 | convolution fusion | flops 270794752 | bytes 2630144 | tf_op jit(solution)/shard_map/while/body/eval_jaxpr/hts,shd->thd/dot_general | solution.py:45
  77.7 0.7 fusion.55
  78.4 0.7 fusion.54
  79.1 0.7 fusion.53
  79.7 0.7 fusion.52
  80.4 0.7 fusion.51
  81.1 0.7 fusion.50
  81.7 0.7 fusion.49
  82.4 0.7 fusion.48
  83.1 3.6 %all-to-all-start.2 = ((bf16[8,1,512,128]{3,2,1,0:T(8,128)(2,1)}), bf16[8,1,512,128]{3,2,1,0:T(8,128)(2,1)S(1)}, u32[]{:S(2)}, u32[]{:S(2)}) async-start(bf16[8,1,512,128]{3,2,1,0:T(8,128)(2,1)} %fusion.48), calls=%async_computation.2 | async-start | bytes 2097152 | tf_op jit(solution)/shard_map/all_to_all | solution.py:53
  87.2 25.2 %all-to-all-done.2 = bf16[8,1,512,128]{3,2,1,0:T(8,128)(2,1)S(1)} async-done(((bf16[8,1,512,128]{3,2,1,0:T(8,128)(2,1)}), bf16[8,1,512,128]{3,2,1,0:T(8,128)(2,1)S(1)}, u32[]{:S(2)}, u32[]{:S(2)}) %all-to-all-start.2) | async-done | bytes 1048608 | tf_op jit(solution)/shard_map/all_to_all | solution.py:53
  112.4 1.5 %convert_bitcast_fusion = f32[1,512,8,128]{3,1,0,2:T(8,128)} fusion(bf16[8,1,512,128]{3,2,1,0:T(8,128)(2,1)S(1)} %all-to-all-done.2), kind=kLoop, calls=%fused_computation.47 | loop fusion | flops 524288 | bytes 3145728 | tf_op jit(solution)/shard_map/convert_element_type | solution.py:56
  113.9 1.9 %copy.54 = f32[1,512,8,128]{1,3,2,0:T(8,128)S(1)} copy(f32[1,512,8,128]{3,1,0,2:T(8,128)} %convert_bitcast_fusion) | data formatting | bytes 4194304 | tf_op jit(solution)/shard_map/convert_element_type | solution.py:56
  115.8 1.8 %fusion.46 = bf16[1,512,1024]{1,2,0:T(8,128)(2,1)} fusion(bf16[1,512,1024]{1,2,0:T(8,128)(2,1)S(1)} %copy.44, f32[1,512,8,128]{1,3,2,0:T(8,128)S(1)} %copy.54), kind=kLoop, calls=%fused_computation.46 | loop fusion | flops 5767168 | bytes 4194304 | tf_op jit(solution)/shard_map/convert_element_type | solution.py:56
  117.6 2.3 %copy.55 = bf16[1,512,1024]{2,1,0:T(8,128)(2,1)} copy(bf16[1,512,1024]{1,2,0:T(8,128)(2,1)} %fusion.46) | data formatting | bytes 2097152 | tf_op jit(solution)/shard_map/convert_element_type | solution.py:56
  (36 shorter events, 2.9 us)
Async XLA Ops:
  6.5 59.7 %all-gather.2.cloned.1.call-start = ((), (), s32[]{:S(2)}) async-start(), calls=%async_computation.3 | async-start | bytes 2621440 | tf_op jit(solution)/shard_map/all_gather | solution.py:38
  9.8 20.6 %all-to-all-start.1 = ((bf16[8,2,256]{2,1,0:T(2,128)(2,1)}), bf16[8,2,256]{2,1,0:T(2,128)(2,1)S(1)}, u32[]{:S(2)}, u32[]{:S(2)}) async-start(bf16[8,2,256]{2,1,0:T(2,128)(2,1)} %reshape.282), calls=%async_computation.1 | async-start | bytes 16384 | tf_op jit(solution)/shard_map/all_to_all | solution.py:29
  28.7 7.6 %copy-start.3 = (bf16[128]{0:T(256)(128)(2,1)S(1)}, bf16[128]{0:T(256)(128)(2,1)}, u32[]{:S(2)}) copy-start(bf16[128]{0:T(256)(128)(2,1)} %param.11) | copy-start | bytes 772
  28.8 7.6 %copy-start.2 = (bf16[1,1024]{1,0:T(2,128)(2,1)S(1)}, bf16[1,1024]{1,0:T(2,128)(2,1)}, u32[]{:S(2)}) copy-start(bf16[1,1024]{1,0:T(2,128)(2,1)} %param.13) | copy-start | bytes 6148
  30.4 31.4 %all-to-all-start = ((bf16[8,2,32768]{2,1,0:T(2,128)(2,1)}), bf16[8,2,32768]{2,1,0:T(2,128)(2,1)S(1)}, u32[]{:S(2)}, u32[]{:S(2)}) async-start(bf16[8,2,32768]{2,1,0:T(2,128)(2,1)} %reshape.280), calls=%async_computation | async-start | bytes 2097152 | tf_op jit(solution)/shard_map/all_to_all | solution.py:28
  64.5 1.7 %copy-start = (bf16[4,1024,1,128]{3,1,0,2:T(8,128)(2,1)S(1)}, bf16[4,1024,1,128]{3,1,0,2:T(8,128)(2,1)}, u32[]{:S(2)}) copy-start(bf16[4,1024,1,128]{3,1,0,2:T(8,128)(2,1)} %custom-call.1) | copy-start | bytes 3145732
  77.7 8.9 %copy-start.1 = (bf16[1,512,1024]{2,1,0:T(8,128)(2,1)S(1)}, bf16[1,512,1024]{2,1,0:T(8,128)(2,1)}, u32[]{:S(2)}) copy-start(bf16[1,512,1024]{2,1,0:T(8,128)(2,1)} %param.8) | copy-start | bytes 3145732
  83.1 29.3 %all-to-all-start.2 = ((bf16[8,1,512,128]{3,2,1,0:T(8,128)(2,1)}), bf16[8,1,512,128]{3,2,1,0:T(8,128)(2,1)S(1)}, u32[]{:S(2)}, u32[]{:S(2)}) async-start(bf16[8,1,512,128]{3,2,1,0:T(8,128)(2,1)} %fusion.48), calls=%async_computation.2 | async-start | bytes 2097152 | tf_op jit(solution)/shard_map/all_to_all | solution.py:53
Sparse Core Ops, SparseCore 0:
  8.9 25.2 all-gather.1
